TPU v7x, 32 devices: a whole 2x2x4 slice. The times are simulated.
32 devices in a mesh: sp: 8 (over z, x), tp: 4 (over y, core).
Axes of the slice: x: 2, y: 2, z: 4, core: 2. Of those that a mesh axis runs over, the one named last changes fastest.
Arguments:
- residual_in: bfloat16 [2048, 2048], P(('sp', 'tp')), may hold values from -0.119628906 to 0.119628906
- queries: bfloat16 [2048, 2048], P('sp', 'tp'), may hold values from -6 to 6
- keys_raw: bfloat16 [2048, 512], P('sp', 'tp'), may hold values from -6 to 6
- values_raw: bfloat16 [2048, 512], P('sp', 'tp'), may hold values from -6 to 6
- query_gain: float32 [128], replicated, may hold values from 0.28 to 7
- key_gain: float32 [128], replicated, may hold values from 0.28 to 7
- out_weight: bfloat16 [2048, 2048], P('tp'), may hold values from -0.125 to 0.125
- norm_gain: float32 [2048], replicated, may hold values from 0.1 to 1.9
- gate_weight: bfloat16 [2048, 5632], P('sp', 'tp'), may hold values from -0.125 to 0.125
- up_weight: bfloat16 [2048, 5632], P('sp', 'tp'), may hold values from -0.125 to 0.125
- down_weight: bfloat16 [5632, 2048], P('tp', 'sp'), may hold values from -0.078125 to 0.078125
Outputs:
- residual_out: bfloat16 [2048, 2048], P(('sp', 'tp'))
All inputs are finite; a program needn't handle non-finite values.
Results may differ from a plain program's by a relative error of at most 0.024.
The roundings to bfloat16 on the way count: a program that leaves them out, or rounds other values in their place, can miss the bound.
Values may be sent and summed in bfloat16 or wider, within the bound.
A program may use at most 128 MiB of HBM per device.

v0:
```python
import jax
import jax.numpy as jnp
from jax import lax
from jax.sharding import PartitionSpec as P

GRID_W = 64
EPS = 1e-06
THETA = 10000.0


def turn_half(part, angles):
    quarter = part.shape[-1] // 2
    cosine = jnp.cos(angles)[:, None, :]
    sine = jnp.sin(angles)[:, None, :]
    first = part[..., :quarter]
    second = part[..., quarter:]
    return part * cosine + jnp.concatenate([-second, first], axis=-1) * sine


def prepare_heads(raw, gain, positions, heads):
    count = raw.shape[0]
    head_dim = gain.shape[0]
    half = head_dim // 2
    vec = raw.astype(jnp.float32).reshape(count, heads, head_dim)
    vec = vec * lax.rsqrt(jnp.mean(vec * vec, axis=-1, keepdims=True) + EPS) * gain
    freqs = THETA ** (-jnp.arange(0, half, 2, dtype=jnp.float32) / half)
    row_ang = (positions // GRID_W).astype(jnp.float32)[:, None] * freqs
    col_ang = (positions % GRID_W).astype(jnp.float32)[:, None] * freqs
    row_ang = jnp.concatenate([row_ang, row_ang], axis=-1)
    col_ang = jnp.concatenate([col_ang, col_ang], axis=-1)
    turned = jnp.concatenate(
        [turn_half(vec[..., :half], row_ang), turn_half(vec[..., half:], col_ang)], axis=-1
    )
    return turned.astype(jnp.bfloat16)


def per_device(
    residual_in,
    queries,
    keys_raw,
    values_raw,
    query_gain,
    key_gain,
    out_weight,
    norm_gain,
    gate_weight,
    up_weight,
    down_weight,
):
    tok = queries.shape[0]
    head_dim = query_gain.shape[0]
    local_heads = queries.shape[1] // head_dim
    local_kv = keys_raw.shape[1] // head_dim
    group = local_heads // local_kv
    gate_full, up_full = (
        lax.all_gather(gate_weight, "sp", axis=0, tiled=True),
        lax.all_gather(up_weight, "sp", axis=0, tiled=True),
    )
    down_full = lax.all_gather(down_weight, "sp", axis=1, tiled=True)
    positions = lax.axis_index("sp") * tok + jnp.arange(tok, dtype=jnp.int32)
    q_rot = prepare_heads(queries, query_gain, positions, local_heads).reshape(
        tok, local_kv, group, head_dim
    )
    k_rot = prepare_heads(keys_raw, key_gain, positions, local_kv)
    vals = values_raw.reshape(tok, local_kv, head_dim)
    start_state = (
        jnp.full((tok, local_kv, group), -jnp.inf, jnp.float32),
        jnp.zeros((tok, local_kv, group), jnp.float32),
        jnp.zeros((tok, local_kv, group, head_dim), jnp.float32),
    )
    carry = start_state
    k_piece = lax.all_gather(k_rot, "sp", axis=0, tiled=True)
    v_piece = lax.all_gather(vals, "sp", axis=0, tiled=True)
    length = k_piece.shape[0]
    shards = length // tok
    per_step = max(1, 2048 // tok)
    factor = max((d for d in range(1, shards + 1) if shards % d == 0 and d <= per_step))
    span = factor * tok
    k_blocks = k_piece.reshape(length // span, span, local_kv, head_dim)
    v_blocks = v_piece.reshape(length // span, span, local_kv, head_dim)

    def step(state, blocks):
        top, total, summed = state
        k_blk, v_blk = blocks
        scores = jnp.einsum(
            "qkgd,skd->qkgs", q_rot, k_blk, preferred_element_type=jnp.float32
        ) * head_dim ** (-0.5)
        new_top = jnp.maximum(top, jnp.max(scores, axis=-1))
        shrink = jnp.exp(top - new_top)
        expo = jnp.exp(scores - new_top[..., None])
        total = total * shrink + jnp.sum(expo, axis=-1)
        summed = summed * shrink[..., None] + jnp.einsum(
            "qkgs,skd->qkgd", expo.astype(jnp.bfloat16), v_blk, preferred_element_type=jnp.float32
        )
        return ((new_top, total, summed), None)

    carry, _ = lax.scan(step, carry, (k_blocks, v_blocks))
    top, total, summed = carry
    attended = (summed / total[..., None]).astype(jnp.bfloat16).reshape(tok, local_heads * head_dim)
    projected = lax.psum_scatter(
        jnp.dot(attended, out_weight, preferred_element_type=jnp.float32).astype(jnp.bfloat16),
        "tp",
        scatter_dimension=0,
        tiled=True,
    ).astype(jnp.float32)
    mixed = (residual_in.astype(jnp.float32) + projected).astype(jnp.bfloat16)
    mixed_f = mixed.astype(jnp.float32)
    normed = (
        mixed_f * lax.rsqrt(jnp.mean(mixed_f * mixed_f, axis=-1, keepdims=True) + EPS) * norm_gain
    ).astype(jnp.bfloat16)
    whole_rows = lax.all_gather(normed, "tp", axis=0, tiled=True)
    gate = jnp.dot(whole_rows, gate_full, preferred_element_type=jnp.float32)
    up_val = jnp.dot(whole_rows, up_full, preferred_element_type=jnp.float32)
    hidden = (jax.nn.silu(gate) * up_val).astype(jnp.bfloat16)
    terms = jnp.dot(hidden, down_full, preferred_element_type=jnp.float32)
    fed = lax.psum_scatter(
        terms.astype(jnp.bfloat16), "tp", scatter_dimension=0, tiled=True
    ).astype(jnp.float32)
    return (mixed_f + 0.5 * fed).astype(jnp.bfloat16)


def solution(mesh):
    placed = (
        P(("sp", "tp"), None),
        P("sp", "tp"),
        P("sp", "tp"),
        P("sp", "tp"),
        P(),
        P(),
        P("tp", None),
        P(),
        P("sp", "tp"),
        P("sp", "tp"),
        P("tp", "sp"),
    )
    return jax.shard_map(
        per_device, mesh=mesh, in_specs=placed, out_specs=P(("sp", "tp"), None), check_vma=False
    )
```

profile of v0, /device:TPU:0, one launch (start us, length us, event | category | flops | bytes accessed | tf_op | source)
XLA Modules:
  0.0 460.9 jit_solution(13443270139341550448)
XLA Ops:
  6.5 0.0 reduce-scatter.3.cloned.1.call-start
  6.6 1.1 fusion.33
  7.7 0.9 fusion.35
  8.6 0.2 slice_negate_fusion.3
  8.8 0.8 broadcast_multiply_fusion.1
  9.6 1.2 fusion.39
  10.8 0.1 pad_maximum_fusion.4
  10.9 33.0 %all_gather.18 = bf16[2048,1,128]{2,0,1:T(8,128)(2,1)S(1)} all-gather(bf16[256,1,128]{2,0,1:T(8,128)(2,1)S(1)} %pad_maximum_fusion.4), channel_id=1, replica_groups=mesh['sp'=8,'tp'=4] {'sp'}, dimensions={0}, use_global_device_ids=true | all-gather | bytes 589824 | tf_op jit(solution)/shard_map/all_gather | solution.py:72
  43.9 1.1 copy.14
  45.0 0.1 multiply_reduce_fusion
  45.1 0.1 copy.15
  45.2 0.9 multiply_multiply_fusion
  46.1 0.5 slice_negate_fusion.1
  46.6 1.5 fusion.43
  48.1 0.5 fusion.41
  48.7 0.5 fusion.26
  49.1 1.3 bitcast_reduce_fusion
  50.5 0.0 copy-start.4
  50.5 3.2 copy-done.1
  53.7 1.4 fusion.1
  55.1 0.0 copy-done.4
  55.1 0.1 copy.16
  55.2 31.3 %all-gather = bf16[2048,128]{0,1:T(8,128)(2,1)S(1)} all-gather(bf16[256,128]{0,1:T(8,128)(2,1)S(1)} %copy.16), channel_id=2, replica_groups=mesh['sp'=8,'tp'=4] {'sp'}, dimensions={0}, use_global_device_ids=true | all-gather | bytes 589824 | tf_op jit(solution)/shard_map/all_gather | solution.py:73
  86.5 5.1 %fusion.16 = bf16[1,128,256,4]{2,1,3,0:T(8,128)(2,1)S(1)} fusion(f32[2048,256,4]{1,0,2:T(8,128)} %copy-done.1, f32[256,4]{0,1:T(4,128)S(1)} %get-tuple-element.50, bf16[2048,128]{0,1:T(8,128)(2,1)S(1)} %all-gather, f32[256,4]{0,1:T(4,128)S(1)} %get-tuple-element.43, f32[256,4]{0,1:T(4,128)S(1)} %get-tuple-element.42), kind=kOutput, calls=%fused_computation.14 | convolution fusion | flops 543555584 | bytes 9187328 | tf_op jit(solution)/shard_map/while/body/eval_jaxpr/qkgs,skd->qkgd/dot_general | solution.py:92
  91.6 1.7 convolution_convert_fusion
  93.3 0.0 reduce-scatter.3.cloned.1.call-update
  93.3 0.0 all-gather.6.cloned.1.call-start
  93.4 26.1 %reduce-scatter.3.cloned.1.call-done = bf16[64,2048]{1,0:T(8,128)(2,1)} async-done(((bf16[256,2048]{1,0:T(8,128)(2,1)}), bf16[64,2048]{1,0:T(8,128)(2,1)}) %reduce-scatter.3.cloned.1.call-update) | async-done | bytes 262160 | tf_op jit(solution)/shard_map/reduce_scatter | solution.py:100
  119.4 1.1 fusion.19
  120.6 0.0 copy-done.5
  120.6 1.8 fusion.21
  122.4 0.0 all-gather.6.cloned.1.call-update
  122.4 0.0 all-gather.8.cloned.1.call-start
  122.5 0.7 all-gather.8.cloned.1.call-update
  123.1 0.0 all-gather.10.cloned.1.call-start
  123.2 0.5 all-gather.10.cloned.1.call-update
  123.7 0.0 all-gather.12.cloned.1.call-start
  123.8 0.5 all-gather.12.cloned.1.call-update
  124.3 0.2 reduce-scatter.5.cloned.1.call-start
  124.5 14.7 %all-gather.6.cloned.1.call-done = bf16[256,2048]{1,0:T(8,128)(2,1)} async-done(((bf16[64,2048]{1,0:T(8,128)(2,1)}), bf16[256,2048]{1,0:T(8,128)(2,1)}) %all-gather.6.cloned.1.call-update) | async-done | bytes 1048592 | tf_op jit(solution)/shard_map/all_gather | solution.py:111
  139.3 94.5 %all-gather.8.cloned.1.call-done = bf16[2048,1408]{1,0:T(8,128)(2,1)} async-done(((bf16[256,1408]{1,0:T(8,128)(2,1)}), bf16[2048,1408]{1,0:T(8,128)(2,1)}) %all-gather.8.cloned.1.call-update) | async-done | bytes 5767184 | tf_op jit(solution)/shard_map/all_gather | solution.py:56
  233.8 5.9 %fusion.53 = f32[256,1408]{1,0:T(8,128)} fusion(bf16[256,2048]{1,0:T(8,128)(2,1)} %all-gather.6.cloned.1.call-done, bf16[2048,1408]{1,0:T(8,128)(2,1)} %all-gather.8.cloned.1.call-done), kind=kOutput, calls=%fused_computation.88 | convolution fusion | flops 1476395008 | bytes 8257536 | tf_op jit(solution)/shard_map/dot_general | solution.py:112
  239.7 86.7 %all-gather.10.cloned.1.call-done = bf16[2048,1408]{1,0:T(8,128)(2,1)} async-done(((bf16[256,1408]{1,0:T(8,128)(2,1)}), bf16[2048,1408]{1,0:T(8,128)(2,1)}) %all-gather.10.cloned.1.call-update) | async-done | bytes 5767184 | tf_op jit(solution)/shard_map/all_gather | solution.py:57
  326.3 93.2 %all-gather.12.cloned.1.call-done = bf16[1408,2048]{1,0:T(8,128)(2,1)} async-done(((bf16[1408,256]{1,0:T(8,128)(2,1)}), bf16[1408,2048]{1,0:T(8,128)(2,1)}) %all-gather.12.cloned.1.call-update) | async-done | bytes 5767184 | tf_op jit(solution)/shard_map/all_gather | solution.py:59
  419.6 9.5 %convolution_convert_fusion.1 = bf16[256,2048]{1,0:T(8,128)(2,1)} fusion(bf16[1408,2048]{1,0:T(8,128)(2,1)} %all-gather.12.cloned.1.call-done, bf16[256,2048]{1,0:T(8,128)(2,1)} %all-gather.6.cloned.1.call-done, bf16[2048,1408]{1,0:T(8,128)(2,1)} %all-gather.10.cloned.1.call-done, f32[256,1408]{1,0:T(8,128)} %fusion.53), kind=kOutput, calls=%fused_computation.10 | convolution fusion | flops 2955476992 | bytes 15073280 | tf_op jit(solution)/shard_map/dot_general | solution.py:115
  429.1 0.0 reduce-scatter.5.cloned.1.call-update
  429.1 23.1 %reduce-scatter.5.cloned.1.call-done = bf16[64,2048]{1,0:T(8,128)(2,1)} async-done(((bf16[256,2048]{1,0:T(8,128)(2,1)}), bf16[64,2048]{1,0:T(8,128)(2,1)}) %reduce-scatter.5.cloned.1.call-update) | async-done | bytes 262160 | tf_op jit(solution)/shard_map/reduce_scatter | solution.py:116
  452.3 1.8 fusion.22
  (14 shorter events, 0.1 us)
Async XLA Ops:
  6.5 85.0 %copy-start = (bf16[512,2048]{1,0:T(8,128)(2,1)S(1)}, bf16[512,2048]{1,0:T(8,128)(2,1)}, u32[]{:S(2)}) copy-start(bf16[512,2048]{1,0:T(8,128)(2,1)} %param.17) | copy-start | bytes 6291460
  6.5 112.9 %reduce-scatter.3.cloned.1.call-start = ((), (), s32[]{:S(2)}) async-start(), calls=%async_computation.2 | async-start | bytes 1310720 | tf_op jit(solution)/shard_map/reduce_scatter | solution.py:100
  50.5 3.2 copy-start.1
  50.5 4.6 %copy-start.4 = (bf16[256,128]{1,0:T(8,128)(2,1)S(1)}, bf16[256,128]{1,0:T(8,128)(2,1)}, u32[]{:S(2)}) copy-start(bf16[256,128]{1,0:T(8,128)(2,1)} %param.14) | copy-start | bytes 196612
  86.5 32.9 %copy-start.2 = (bf16[64,2048]{1,0:T(8,128)(2,1)S(1)}, bf16[64,2048]{1,0:T(8,128)(2,1)}, u32[]{:S(2)}) copy-start(bf16[64,2048]{1,0:T(8,128)(2,1)} %param.11) | copy-start | bytes 786436
  86.5 34.1 %copy-start.5 = (f32[2048]{0:T(1024)S(1)}, f32[2048]{0:T(1024)}, u32[]{:S(2)}) copy-start(f32[2048]{0:T(1024)} %param.18) | copy-start | bytes 24580
  93.3 45.9 %all-gather.6.cloned.1.call-start = ((), (), s32[]{:S(2)}) async-start(), calls=%async_computation.3 | async-start | bytes 1310720 | tf_op jit(solution)/shard_map/all_gather | solution.py:111
  122.4 111.4 %all-gather.8.cloned.1.call-start = ((), (), s32[]{:S(2)}) async-start(), calls=%async_computation.4 | async-start | bytes 6488064 | tf_op jit(solution)/shard_map/all_gather | solution.py:56
  123.1 203.2 %all-gather.10.cloned.1.call-start = ((), (), s32[]{:S(2)}) async-start(), calls=%async_computation.5 | async-start | bytes 6488064 | tf_op jit(solution)/shard_map/all_gather | solution.py:57
  123.7 295.9 %all-gather.12.cloned.1.call-start = ((), (), s32[]{:S(2)}) async-start(), calls=%async_computation.6 | async-start | bytes 6488064 | tf_op jit(solution)/shard_map/all_gather | solution.py:59
  124.3 327.9 %reduce-scatter.5.cloned.1.call-start = ((), (), s32[]{:S(2)}) async-start(), calls=%async_computation.7 | async-start | bytes 1310720 | tf_op jit(solution)/shard_map/reduce_scatter | solution.py:116
  239.7 212.6 %copy-start.3 = (bf16[64,2048]{1,0:T(8,128)(2,1)S(1)}, bf16[64,2048]{1,0:T(8,128)(2,1)}, u32[]{:S(2)}) copy-start(bf16[64,2048]{1,0:T(8,128)(2,1)} %reduce-scatter.3.cloned.1.call-done) | copy-start | bytes 786436
Sparse Core Ops, SparseCore 0:
  93.4 25.9 reduce-scatter.2
  122.5 16.6 all-gather.5
  141.4 92.2 all-gather.7
  235.8 90.4 all-gather.9
  328.2 91.2 all-gather.11
  429.2 22.9 reduce-scatter.4
where the time goes:
time: 461 us
  waiting for transfers between devices  340 us (74%)
  blocking collectives  64.3 us (14%)
  matrix products  23.5 us (5%)
  other arithmetic  14.3 us (3%)
  between operations  13.6 us (3%)
    all_gather x1, waiting for transfers between devices, per_device(): lax.all_gather(gate_weight, 'sp', axis=0, tiled=True)  94.5 us
    all_gather x1, waiting for transfers between devices, per_device(): down_full = lax.all_gather(down_weight, 'sp', axis=1, tiled=True)  93.2 us
    all_gather x1, waiting for transfers between devices, per_device(): lax.all_gather(up_weight, 'sp', axis=0, tiled=True)  86.7 us
    all_gather x1, blocking collectives, per_device(): k_piece = lax.all_gather(k_rot, 'sp', axis=0, tiled=True)  33 us
    all_gather x1, blocking collectives, per_device(): v_piece = lax.all_gather(vals, 'sp', axis=0, tiled=True)  31.3 us
    reduce_scatter x1, waiting for transfers between devices, per_device(): lax.psum_scatter(jnp.dot(attended, out_weight, preferred_element_type=jnp...  26.1 us
    reduce_scatter x1, waiting for transfers between devices, per_device(): lax.psum_scatter(terms.astype(jnp.bfloat16), 'tp', scatter_dimension=0, t...  23.1 us
    all_gather x1, waiting for transfers between devices, per_device(): whole_rows = lax.all_gather(normed, 'tp', axis=0, tiled=True)  14.7 us
  transfers between devices with their start and end apart: 6, of which 6 were waited for; matrix products, arithmetic and copies ran while one was open for 1% of the time, Pallas kernels for 0%

commit v1 on v0

--- a/solution.py
+++ b/solution.py
@@ -69,8 +69,11 @@
         jnp.zeros((tok, local_kv, group, head_dim), jnp.float32),
     )
     carry = start_state
-    k_piece = lax.all_gather(k_rot, "sp", axis=0, tiled=True)
-    v_piece = lax.all_gather(vals, "sp", axis=0, tiled=True)
+    k_piece, v_piece = jnp.split(
+        lax.all_gather(jnp.concatenate([k_rot, vals], axis=1), "sp", axis=0, tiled=True),
+        [k_rot.shape[1]],
+        axis=1,
+    )
     length = k_piece.shape[0]
     shards = length // tok
     per_step = max(1, 2048 // tok)

time: 461 us -> 427 us (0.926)
  blocking collectives: 64.3 us -> 0 us
  waiting for transfers between devices: 340 us -> 377 us
    all_gather x2 -> x0, blocking collectives: 64.3 us -> none  [the longest x1 33 us: per_device(): k_piece = lax.all_gather(k_rot, 'sp', axis=0, tiled=True)]
    all_gather x0 -> x1, waiting for transfers between devices: none -> 39.5 us  [per_device(): lax.all_gather(jnp.concatenate([k_rot, vals], axis=1), 'sp', axis=0, tile...]
  transfers between devices with their start and end apart: 6 -> 7, of which waited for: 6 -> 7; matrix products, arithmetic and copies ran while one was open for 1% -> 2% of each run, Pallas kernels for 0% -> 0%
where the time goes in v1:
time: 427 us
  waiting for transfers between devices  377 us (88%)
  matrix products  21.2 us (5%)
  between operations  13.7 us (3%)
  other arithmetic  13.5 us (3%)
    all_gather x1, waiting for transfers between devices, per_device(): lax.all_gather(gate_weight, 'sp', axis=0, tiled=True)  94.4 us
    all_gather x1, waiting for transfers between devices, per_device(): down_full = lax.all_gather(down_weight, 'sp', axis=1, tiled=True)  93.2 us
    all_gather x1, waiting for transfers between devices, per_device(): lax.all_gather(up_weight, 'sp', axis=0, tiled=True)  86.6 us
    all_gather x1, waiting for transfers between devices, per_device(): lax.all_gather(jnp.concatenate([k_rot, vals], axis=1), 'sp', axis=0, tile...  39.5 us
    reduce_scatter x1, waiting for transfers between devices, per_device(): lax.psum_scatter(jnp.dot(attended, out_weight, preferred_element_type=jnp...  23.6 us
    reduce_scatter x1, waiting for transfers between devices, per_device(): lax.psum_scatter(terms.astype(jnp.bfloat16), 'tp', scatter_dimension=0, t...  23.1 us
    all_gather x1, waiting for transfers between devices, per_device(): whole_rows = lax.all_gather(normed, 'tp', axis=0, tiled=True)  14.9 us
    dot_general x1, matrix products, per_device(): terms = jnp.dot(hidden, down_full, preferred_element_type=jnp.float32)  9.52 us
  transfers between devices with their start and end apart: 7, of which 7 were waited for; matrix products, arithmetic and copies ran while one was open for 2% of the time, Pallas kernels for 0%

profile of v1, /device:TPU:0, one launch (start us, length us, event | category | flops | bytes accessed | tf_op | source)
XLA Modules:
  0.0 427.1 jit_solution(215766446615522599)
XLA Ops:
  6.6 1.1 fusion.31
  7.7 0.9 fusion.33
  8.6 0.2 slice_negate_fusion.3
  8.8 0.1 broadcast_multiply_fusion.1
  8.9 1.2 fusion.37
  10.2 1.6 pad_maximum_fusion.2
  11.8 0.0 all-gather.6.cloned.1.call-update
  11.8 0.0 reduce-scatter.3.cloned.1.call-start
  11.8 1.1 copy.14
  12.9 0.1 copy.15
  13.1 0.5 fusion.41
  13.6 0.5 fusion.39
  14.2 0.1 multiply_reduce_fusion
  14.2 0.0 copy-done.5
  14.2 0.2 multiply_multiply_fusion
  14.5 0.5 slice_negate_fusion.1
  14.9 0.5 fusion.26
  15.4 39.5 %all-gather.6.cloned.1.call-done = bf16[2048,2,128]{2,0,1:T(8,128)(2,1)} async-done(((bf16[256,2,128]{2,0,1:T(8,128)(2,1)}), bf16[2048,2,128]{2,0,1:T(8,128)(2,1)}) %all-gather.6.cloned.1.call-update) | async-done | bytes 1048592 | tf_op jit(solution)/shard_map/all_gather | solution.py:73
  54.9 2.4 bitcast_reduce_fusion
  57.3 1.4 fusion.1
  58.7 0.0 copy-start.1
  58.7 0.0 copy-start.4
  58.7 1.7 fusion.16
  60.4 1.7 convolution_convert_fusion
  62.1 0.0 reduce-scatter.3.cloned.1.call-update
  62.2 0.0 all-gather.8.cloned.1.call-start
  62.2 23.6 %reduce-scatter.3.cloned.1.call-done = bf16[64,2048]{1,0:T(8,128)(2,1)} async-done(((bf16[256,2048]{1,0:T(8,128)(2,1)}), bf16[64,2048]{1,0:T(8,128)(2,1)}) %reduce-scatter.3.cloned.1.call-update) | async-done | bytes 262160 | tf_op jit(solution)/shard_map/reduce_scatter | solution.py:103
  85.8 1.1 fusion.19
  87.0 0.0 copy-done.4
  87.0 1.8 fusion.21
  88.8 0.0 all-gather.8.cloned.1.call-update
  88.8 0.0 all-gather.10.cloned.1.call-start
  88.8 0.5 all-gather.10.cloned.1.call-update
  89.4 0.0 all-gather.12.cloned.1.call-start
  89.4 0.5 all-gather.12.cloned.1.call-update
  90.0 0.0 all-gather.14.cloned.1.call-start
  90.0 0.5 all-gather.14.cloned.1.call-update
  90.5 0.2 reduce-scatter.5.cloned.1.call-start
  90.8 14.9 %all-gather.8.cloned.1.call-done = bf16[256,2048]{1,0:T(8,128)(2,1)} async-done(((bf16[64,2048]{1,0:T(8,128)(2,1)}), bf16[256,2048]{1,0:T(8,128)(2,1)}) %all-gather.8.cloned.1.call-update) | async-done | bytes 1048592 | tf_op jit(solution)/shard_map/all_gather | solution.py:114
  105.6 94.4 %all-gather.10.cloned.1.call-done = bf16[2048,1408]{1,0:T(8,128)(2,1)} async-done(((bf16[256,1408]{1,0:T(8,128)(2,1)}), bf16[2048,1408]{1,0:T(8,128)(2,1)}) %all-gather.10.cloned.1.call-update) | async-done | bytes 5767184 | tf_op jit(solution)/shard_map/all_gather | solution.py:56
  200.0 5.9 %fusion.51 = f32[256,1408]{1,0:T(8,128)} fusion(bf16[256,2048]{1,0:T(8,128)(2,1)} %all-gather.8.cloned.1.call-done, bf16[2048,1408]{1,0:T(8,128)(2,1)} %all-gather.10.cloned.1.call-done), kind=kOutput, calls=%fused_computation.88 | convolution fusion | flops 1476395008 | bytes 8257536 | tf_op jit(solution)/shard_map/dot_general | solution.py:115
  205.9 86.6 %all-gather.12.cloned.1.call-done = bf16[2048,1408]{1,0:T(8,128)(2,1)} async-done(((bf16[256,1408]{1,0:T(8,128)(2,1)}), bf16[2048,1408]{1,0:T(8,128)(2,1)}) %all-gather.12.cloned.1.call-update) | async-done | bytes 5767184 | tf_op jit(solution)/shard_map/all_gather | solution.py:57
  292.6 93.2 %all-gather.14.cloned.1.call-done = bf16[1408,2048]{1,0:T(8,128)(2,1)} async-done(((bf16[1408,256]{1,0:T(8,128)(2,1)}), bf16[1408,2048]{1,0:T(8,128)(2,1)}) %all-gather.14.cloned.1.call-update) | async-done | bytes 5767184 | tf_op jit(solution)/shard_map/all_gather | solution.py:59
  385.8 9.5 %convolution_convert_fusion.1 = bf16[256,2048]{1,0:T(8,128)(2,1)} fusion(bf16[1408,2048]{1,0:T(8,128)(2,1)} %all-gather.14.cloned.1.call-done, bf16[256,2048]{1,0:T(8,128)(2,1)} %all-gather.8.cloned.1.call-done, bf16[2048,1408]{1,0:T(8,128)(2,1)} %all-gather.12.cloned.1.call-done, f32[256,1408]{1,0:T(8,128)} %fusion.51), kind=kOutput, calls=%fused_computation.10 | convolution fusion | flops 2955476992 | bytes 15073280 | tf_op jit(solution)/shard_map/dot_general | solution.py:118
  395.3 0.0 reduce-scatter.5.cloned.1.call-update
  395.4 23.1 %reduce-scatter.5.cloned.1.call-done = bf16[64,2048]{1,0:T(8,128)(2,1)} async-done(((bf16[256,2048]{1,0:T(8,128)(2,1)}), bf16[64,2048]{1,0:T(8,128)(2,1)}) %reduce-scatter.5.cloned.1.call-update) | async-done | bytes 262160 | tf_op jit(solution)/shard_map/reduce_scatter | solution.py:119
  418.5 0.0 copy-done.2
  418.5 1.8 fusion.22
  (14 shorter events, 0.1 us)
Async XLA Ops:
  6.5 53.9 %copy-start = (bf16[512,2048]{1,0:T(8,128)(2,1)S(1)}, bf16[512,2048]{1,0:T(8,128)(2,1)}, u32[]{:S(2)}) copy-start(bf16[512,2048]{1,0:T(8,128)(2,1)} %param.17) | copy-start | bytes 6291460
  6.5 7.7 %copy-start.5 = (f32[128]{0:T(128)S(1)}, f32[128]{0:T(128)}, u32[]{:S(2)}) copy-start(f32[128]{0:T(128)} %param.15) | copy-start | bytes 1540
  6.5 48.4 %all-gather.6.cloned.1.call-start = ((), (), s32[]{:S(2)}) async-start(), calls=%async_computation.2 | async-start | bytes 1179648 | tf_op jit(solution)/shard_map/all_gather | solution.py:73
  11.8 74.0 %reduce-scatter.3.cloned.1.call-start = ((), (), s32[]{:S(2)}) async-start(), calls=%async_computation.3 | async-start | bytes 1310720 | tf_op jit(solution)/shard_map/reduce_scatter | solution.py:103
  57.3 1.4 copy-start.3
  58.7 27.1 %copy-start.1 = (bf16[64,2048]{1,0:T(8,128)(2,1)S(1)}, bf16[64,2048]{1,0:T(8,128)(2,1)}, u32[]{:S(2)}) copy-start(bf16[64,2048]{1,0:T(8,128)(2,1)} %param.11) | copy-start | bytes 786436
  58.7 28.3 %copy-start.4 = (f32[2048]{0:T(1024)S(1)}, f32[2048]{0:T(1024)}, u32[]{:S(2)}) copy-start(f32[2048]{0:T(1024)} %param.18) | copy-start | bytes 24580
  62.2 43.5 %all-gather.8.cloned.1.call-start = ((), (), s32[]{:S(2)}) async-start(), calls=%async_computation.4 | async-start | bytes 1310720 | tf_op jit(solution)/shard_map/all_gather | solution.py:114
  88.8 111.2 %all-gather.10.cloned.1.call-start = ((), (), s32[]{:S(2)}) async-start(), calls=%async_computation.5 | async-start | bytes 6488064 | tf_op jit(solution)/shard_map/all_gather | solution.py:56
  89.4 203.2 %all-gather.12.cloned.1.call-start = ((), (), s32[]{:S(2)}) async-start(), calls=%async_computation.6 | async-start | bytes 6488064 | tf_op jit(solution)/shard_map/all_gather | solution.py:57
  90.0 295.9 %all-gather.14.cloned.1.call-start = ((), (), s32[]{:S(2)}) async-start(), calls=%async_computation.7 | async-start | bytes 6488064 | tf_op jit(solution)/shard_map/all_gather | solution.py:59
  90.5 328.0 %reduce-scatter.5.cloned.1.call-start = ((), (), s32[]{:S(2)}) async-start(), calls=%async_computation.8 | async-start | bytes 1310720 | tf_op jit(solution)/shard_map/reduce_scatter | solution.py:119
  205.9 212.6 %copy-start.2 = (bf16[64,2048]{1,0:T(8,128)(2,1)S(1)}, bf16[64,2048]{1,0:T(8,128)(2,1)}, u32[]{:S(2)}) copy-start(bf16[64,2048]{1,0:T(8,128)(2,1)} %reduce-scatter.3.cloned.1.call-done) | copy-start | bytes 786436
Sparse Core Ops, SparseCore 0:
  11.9 42.9 all-gather.5
  62.3 23.4 reduce-scatter.2
  88.9 16.6 all-gather.7
  107.7 92.2 all-gather.9
  202.0 90.4 all-gather.11
  294.5 91.2 all-gather.13
  395.5 22.9 reduce-scatter.4
